TPU v7x, 32 devices: a whole 2x2x4 slice. The times are simulated.
32 devices in a mesh: grp: 2 (over y), fs: 4 (over z), tp: 4 (over x, core).
Axes of the slice: x: 2, y: 2, z: 4, core: 2. Of those that a mesh axis runs over, the one named last changes fastest.
Arguments:
- tokens: bfloat16 [8, 1024, 2048], P(('grp', 'fs'), None, 'tp'), parts along dimension 0, may hold values from -6 to 6
- mix_gain: float32 [2048], replicated, may hold values from 0.1 to 1.9
- in_matrix: float32 [2048, 1024], P('fs', 'tp'), may hold values from -0.125 to 0.125
- in_scale: float32 [1, 1024], P(None, 'tp'), may hold values from 0.5 to 2
- pool_mix: bfloat16 [8, 128, 128], P('tp'), may hold values from -0.5 to 0.5
- pool_scale: float32 [1, 1024], P(None, 'tp'), may hold values from 0.1 to 1.9
- out_matrix: float32 [1024, 2048], P('tp', 'fs'), may hold values from -0.25 to 0.25
- out_scale: float32 [1, 2048], P(None, 'fs'), may hold values from 0.5 to 2
- ffn_gain: float32 [2048], replicated, may hold values from 0.1 to 1.9
- gate_matrix: float32 [2048, 5632], P('fs', 'tp'), may hold values from -0.125 to 0.125
- gate_scale: float32 [1, 5632], P(None, 'tp'), may hold values from 0.5 to 2
- up_matrix: float32 [2048, 5632], P('fs', 'tp'), may hold values from -0.125 to 0.125
- up_scale: float32 [1, 5632], P(None, 'tp'), may hold values from 0.5 to 2
- gate_taps: float32 [3, 5632], P(None, 'tp'), may hold values from -4 to 4
- up_taps: float32 [3, 5632], P(None, 'tp'), may hold values from -4 to 4
- down_matrix: float32 [5632, 2048], P('tp', 'fs'), may hold values from -0.109375 to 0.109375
- down_scale: float32 [1, 2048], P(None, 'fs'), may hold values from 0.5 to 2
Outputs:
- layer_out: bfloat16 [8, 1024, 2048], P(('grp', 'fs'), None, 'tp'), parts along dimension 0
There are 2 independent parts, one for each index of `grp`. A program takes and returns all parts, laid end to end along the dimension named above; an argument that names none is the same for every part. Nothing has to cross between parts.
All inputs are finite; a program needn't handle non-finite values.
Results may differ from a plain program's by a relative error of at most 0.025.
Values may be sent and summed in bfloat16 or wider, within the bound.
No kernel may reach another device: no remote copies, remote signals or barrier semaphores. Data moves between devices by JAX's collectives and lax.ppermute only.
A program may use at most 128 MiB of HBM per device.

v0:
```python
import jax
import jax.numpy as jnp
from jax import lax
from jax.sharding import PartitionSpec as P

BLOCKS = 8
eps = 1e-06
widest_span = 16


def norm_rows(tok_rows, norm_gain):
    values = tok_rows.astype(jnp.float32)
    scaled = values * lax.rsqrt(jnp.mean(values * values, axis=-1, keepdims=True) + eps)
    return (scaled * norm_gain).astype(jnp.bfloat16)


def span_widths(block_ids):
    return jnp.left_shift(jnp.ones_like(block_ids), 1 + 4 * block_ids // BLOCKS)


def trailing_gap(projected, windows):
    values = projected.astype(jnp.float32)
    length = values.shape[0]
    running = values
    for offset in range(1, widest_span):
        shifted = jnp.pad(values[: length - offset], ((offset, 0), (0, 0)))
        running = running + jnp.where(windows[None, :] > offset, shifted, jnp.zeros_like(shifted))
    positions = jnp.arange(length, dtype=jnp.int32)[:, None]
    counts = jnp.minimum(positions + 1, windows[None, :]).astype(jnp.float32)
    return (running / counts - values).astype(jnp.bfloat16)


def causal_taps(linear, tap_table):
    values = linear.astype(jnp.float32)
    length = values.shape[0]
    back_one = jnp.pad(values[: length - 1], ((1, 0), (0, 0)))
    back_two = jnp.pad(values[: length - 2], ((2, 0), (0, 0)))
    return tap_table[2] * values + tap_table[1] * back_one + tap_table[0] * back_two


def fold_rows(operand, portion):
    return jnp.dot(operand, portion, preferred_element_type=jnp.float32)


def shards(
    tokens,
    mix_gain,
    in_matrix,
    in_scale,
    pool_mix,
    pool_scale,
    out_matrix,
    out_scale,
    ffn_gain,
    gate_matrix,
    gate_scale,
    up_matrix,
    up_scale,
    gate_taps,
    up_taps,
    down_matrix,
    down_scale,
):
    length = tokens.shape[1]
    own_width = tokens.shape[2]
    local_rows = tokens.reshape(length, own_width)
    gathered = lax.all_gather(local_rows, "tp", axis=1, tiled=True)
    normed = norm_rows(gathered, mix_gain)
    width_in = in_matrix.shape[1]
    in_total = fold_rows(
        normed, lax.all_gather(in_matrix.astype(jnp.bfloat16), "fs", axis=0, tiled=True)
    )
    projected = (in_total * in_scale).astype(jnp.bfloat16)
    local_blocks = pool_mix.shape[0]
    block_width = pool_mix.shape[1]
    block_ids = lax.axis_index("tp") * local_blocks + jnp.arange(local_blocks, dtype=jnp.int32)
    windows = jnp.repeat(span_widths(block_ids), block_width)
    spread = trailing_gap(projected, windows)
    block_mixed = jnp.einsum(
        "lbc,bce->lbe",
        spread.reshape(length, local_blocks, block_width),
        pool_mix,
        preferred_element_type=jnp.float32,
    ).reshape(length, width_in)
    pooled = (block_mixed * pool_scale).astype(jnp.bfloat16)
    out_cols = lax.all_gather(out_scale, "fs", axis=1, tiled=True)
    tp_index = lax.axis_index("tp")
    groups = lax.axis_size("tp")
    pooled_all = lax.all_gather(pooled, "tp", axis=1, tiled=True)
    row_block = lax.all_gather(out_matrix.astype(jnp.bfloat16), "fs", axis=1, tiled=True)
    own_matrix = lax.all_to_all(row_block, "tp", split_axis=1, concat_axis=0, tiled=True)
    own_scales = lax.dynamic_slice_in_dim(out_cols, tp_index * own_width, own_width, 1)
    grouped_rows = pooled_all.reshape(length, groups, width_in)
    grouped_matrix = own_matrix.reshape(groups, width_in, own_width)
    pieces = (
        jnp.einsum("lgc,gcd->gld", grouped_rows, grouped_matrix, preferred_element_type=jnp.float32)
        * own_scales[None]
    )
    rounded = lax.optimization_barrier(pieces.astype(jnp.bfloat16))
    mixing = jnp.sum(rounded.astype(jnp.float32), axis=0)
    residual = (local_rows.astype(jnp.float32) + mixing).astype(jnp.bfloat16)
    gathered_ffn = lax.all_gather(residual, "tp", axis=1, tiled=True)
    normed_ffn = norm_rows(gathered_ffn, ffn_gain)
    gate_cast = gate_matrix.astype(jnp.bfloat16)
    up_cast = up_matrix.astype(jnp.bfloat16)
    gate_full, up_full = (
        lax.all_gather(gate_cast, "fs", axis=0, tiled=True),
        lax.all_gather(up_cast, "fs", axis=0, tiled=True),
    )
    gate_total = jnp.dot(normed_ffn, gate_full, preferred_element_type=jnp.float32)
    up_total = jnp.dot(normed_ffn, up_full, preferred_element_type=jnp.float32)
    gate_lin = (gate_total * gate_scale).astype(jnp.bfloat16)
    up_lin = (up_total * up_scale).astype(jnp.bfloat16)
    hidden = (jax.nn.silu(causal_taps(gate_lin, gate_taps)) * causal_taps(up_lin, up_taps)).astype(
        jnp.bfloat16
    )
    down_cols = lax.all_gather(down_scale, "fs", axis=1, tiled=True)
    partial_ffn = (
        jnp.dot(
            hidden,
            lax.all_gather(down_matrix.astype(jnp.bfloat16), "fs", axis=1, tiled=True),
            preferred_element_type=jnp.float32,
        )
        * down_cols
    )
    feed_out = lax.psum_scatter(
        partial_ffn.astype(jnp.bfloat16), "tp", scatter_dimension=1, tiled=True
    ).astype(jnp.float32)
    result = (residual.astype(jnp.float32) + feed_out).astype(jnp.bfloat16)
    return result.reshape(1, length, result.shape[1])


def solution(mesh):
    return jax.shard_map(
        shards,
        mesh=mesh,
        in_specs=(
            P(("grp", "fs"), None, "tp"),
            P(),
            P("fs", "tp"),
            P(None, "tp"),
            P("tp", None, None),
            P(None, "tp"),
            P("tp", "fs"),
            P(None, "fs"),
            P(),
            P("fs", "tp"),
            P(None, "tp"),
            P("fs", "tp"),
            P(None, "tp"),
            P(None, "tp"),
            P(None, "tp"),
            P("tp", "fs"),
            P(None, "fs"),
        ),
        out_specs=P(("grp", "fs"), None, "tp"),
        check_vma=False,
    )
```

profile of v0, /device:TPU:0, one launch (start us, length us, event | category | flops | bytes accessed | tf_op | source)
XLA Modules:
  0.0 573.4 jit_solution(17679194408588764987)
XLA Ops:
  6.5 0.7 all-gather.24.cloned.1.call-update
  7.3 1.8 convert_element_type.120
  9.1 0.0 all-gather.14.cloned.1.call-start
  9.2 1.9 copy.22
  11.1 0.0 all-gather.12.cloned.1.call-start
  11.1 0.1 bitcast_compare_fusion.14
  11.2 0.1 broadcast_bitcast_fusion
  11.3 34.8 %all-gather.24.cloned.1.call-done = bf16[1,1024,2048]{2,1,0:T(8,128)(2,1)} async-done(((bf16[1,1024,512]{2,1,0:T(8,128)(2,1)}), bf16[1,1024,2048]{2,1,0:T(8,128)(2,1)}) %all-gather.24.cloned.1.call-update) | async-done | bytes 4194320 | tf_op jit(solution)/shard_map/all_gather | solution.py:67
  46.1 3.1 fusion.3
  49.2 26.5 %all-gather.10.cloned.1.call-done = bf16[2048,256]{1,0:T(8,128)(2,1)} async-done(((bf16[512,256]{1,0:T(8,128)(2,1)}), bf16[2048,256]{1,0:T(8,128)(2,1)}) %all-gather.10.cloned.1.call-update) | async-done | bytes 1048592 | tf_op jit(solution)/shard_map/all_gather | solution.py:71
  75.7 3.8 fusion.20
  79.5 0.1 slice.107
  79.6 0.1 slice.108
  79.7 0.1 slice.109
  79.7 0.1 slice.110
  79.8 0.1 slice.111
  79.9 0.1 slice.112
  80.0 0.1 slice.113
  80.0 0.1 slice.114
  80.1 3.2 fusion.28
  83.4 0.9 fusion.26
  84.3 20.3 %all-gather.14.cloned.1.call-done = bf16[256,2048]{0,1:T(8,128)(2,1)} async-done(((bf16[256,512]{0,1:T(8,128)(2,1)}), bf16[256,2048]{0,1:T(8,128)(2,1)}) %all-gather.14.cloned.1.call-update) | async-done | bytes 1048592 | tf_op jit(solution)/shard_map/all_gather | solution.py:90
  104.7 2.3 copy.23
  106.9 3.5 all-to-all-start
  110.5 0.0 all-gather.16.cloned.1.call-start
  110.5 11.9 %all_gather.34 = f32[1,2048]{1,0:T(1,128)S(1)} all-gather(f32[1,512]{1,0:T(1,128)S(1)} %copy-done.10), channel_id=1, replica_groups=mesh['grp'=2,'fs'=4,'tp'=4] {'fs'}, dimensions={1}, use_global_device_ids=true | all-gather | bytes 10240 | tf_op jit(solution)/shard_map/all_gather | solution.py:86
  122.5 12.5 %all-to-all-done = bf16[256,4,512]{2,0,1:T(8,128)(2,1)S(1)} async-done(((bf16[256,4,512]{2,0,1:T(8,128)(2,1)}), bf16[256,4,512]{2,0,1:T(8,128)(2,1)S(1)}, u32[]{:S(2)}, u32[]{:S(2)}) %all-to-all-start) | async-done | bytes 1048608 | tf_op jit(solution)/shard_map/all_to_all | solution.py:91
  135.0 2.7 all-gather.12.cloned.1.call-done
  137.6 3.0 multiply_convert_fusion.1
  140.6 0.7 convert_reduce_fusion
  141.3 1.3 fusion.13
  142.7 0.0 all-gather.18.cloned.1.call-start
  142.7 1.3 convert_element_type.133
  144.1 0.0 all-gather.20.cloned.1.call-start
  144.2 3.3 convert_element_type.136
  147.5 1.3 convert_element_type.140
  149.0 12.1 %all_gather.39 = f32[1,2048]{1,0:T(1,128)S(1)} all-gather(f32[1,512]{1,0:T(1,128)S(1)} %copy-done.11), channel_id=1, replica_groups=mesh['grp'=2,'fs'=4,'tp'=4] {'fs'}, dimensions={1}, use_global_device_ids=true | all-gather | bytes 10240 | tf_op jit(solution)/shard_map/all_gather | solution.py:117
  161.1 0.1 slice_reduce_fusion.2
  161.2 14.5 %all-gather.16.cloned.1.call-done = bf16[1024,2048]{1,0:T(8,128)(2,1)} async-done(((bf16[1024,512]{1,0:T(8,128)(2,1)}), bf16[1024,2048]{1,0:T(8,128)(2,1)}) %all-gather.16.cloned.1.call-update) | async-done | bytes 4194320 | tf_op jit(solution)/shard_map/all_gather | solution.py:102
  175.7 3.1 fusion
  178.8 105.1 %all-gather.18.cloned.1.call-done = bf16[2048,1408]{1,0:T(8,128)(2,1)} async-done(((bf16[512,1408]{1,0:T(8,128)(2,1)}), bf16[2048,1408]{1,0:T(8,128)(2,1)}) %all-gather.18.cloned.1.call-update) | async-done | bytes 5767184 | tf_op jit(solution)/shard_map/all_gather | solution.py:107
  283.9 11.9 %fusion.11 = f32[1024,1408]{1,0:T(8,128)} fusion(bf16[2048,1408]{1,0:T(8,128)(2,1)} %all-gather.18.cloned.1.call-done, f32[1408]{0:T(1024)S(1)} %reduce.1, bf16[1024,2048]{1,0:T(8,128)(2,1)} %all-gather.16.cloned.1.call-done, f32[2048]{0:T(1024)S(1)} %copy-done.14, f32[1024]{0:T(1024)S(1)} %add_rsqrt_fusion), kind=kOutput, calls=%fused_computation.20 | convolution fusion | flops 5918294016 | bytes 15746560 | tf_op jit(solution)/shard_map/dot_general | solution.py:110
  295.8 94.7 %all-gather.20.cloned.1.call-done = bf16[2048,1408]{1,0:T(8,128)(2,1)} async-done(((bf16[512,1408]{1,0:T(8,128)(2,1)}), bf16[2048,1408]{1,0:T(8,128)(2,1)}) %all-gather.20.cloned.1.call-update) | async-done | bytes 5767184 | tf_op jit(solution)/shard_map/all_gather | solution.py:108
  390.4 12.0 %fusion.12 = f32[1024,1408]{1,0:T(8,128)} fusion(bf16[2048,1408]{1,0:T(8,128)(2,1)} %all-gather.20.cloned.1.call-done, f32[1408]{0:T(1024)S(1)} %reduce.5, bf16[1024,2048]{1,0:T(8,128)(2,1)} %all-gather.16.cloned.1.call-done, f32[2048]{0:T(1024)S(1)} %copy-done.14, f32[1024]{0:T(1024)S(1)} %add_rsqrt_fusion), kind=kOutput, calls=%fused_computation.21 | convolution fusion | flops 5918294016 | bytes 15746560 | tf_op jit(solution)/shard_map/dot_general | solution.py:111
  402.4 94.6 %all-gather.22.cloned.1.call-done = bf16[1408,2048]{1,0:T(8,128)(2,1)} async-done(((bf16[1408,512]{1,0:T(8,128)(2,1)}), bf16[1408,2048]{1,0:T(8,128)(2,1)}) %all-gather.22.cloned.1.call-update) | async-done | bytes 5767184 | tf_op jit(solution)/shard_map/all_gather | solution.py:121
  497.0 24.6 %multiply_convert_fusion = bf16[1024,2048]{1,0:T(8,128)(2,1)} fusion(bf16[1408,2048]{1,0:T(8,128)(2,1)} %all-gather.22.cloned.1.call-done, f32[2048]{0:T(1024)S(1)} %bitcast.83, f32[1022,1408]{1,0:T(8,128)} %bitcast.89, f32[1023,1408]{1,0:T(8,128)} %bitcast.90, f32[1024,1408]{1,0:T(8,128)} %fusion.12, f32[1022,1408]{1,0:T(8,128)} %bitcast.87, ...), kind=kOutput, calls=%fused_computation.10 | convolution fusion | flops 5932843008 | bytes 44572672 | tf_op jit(solution)/shard_map/dot_general | solution.py:119
  521.6 42.8 %reduce-scatter.2.cloned.1.call-done = bf16[1024,512]{1,0:T(8,128)(2,1)} async-done(((bf16[1024,2048]{1,0:T(8,128)(2,1)}), bf16[1024,512]{1,0:T(8,128)(2,1)}) %reduce-scatter.2.cloned.1.call-update) | async-done | bytes 1048592 | tf_op jit(solution)/shard_map/reduce_scatter | solution.py:126
  564.4 2.5 fusion.25
  (51 shorter events, 0.4 us)
Async XLA Ops:
  6.5 73.6 %copy-start = (bf16[2,128,128]{2,1,0:T(8,128)(2,1)S(1)}, bf16[2,128,128]{2,1,0:T(8,128)(2,1)}, u32[]{:S(2)}) copy-start(bf16[2,128,128]{2,1,0:T(8,128)(2,1)} %param.21) | copy-start | bytes 196612
  6.5 69.2 %copy-start.15 = (f32[1,256]{1,0:T(1,128)S(1)}, f32[1,256]{1,0:T(1,128)}, u32[]{:S(2)}) copy-start(f32[1,256]{1,0:T(1,128)} %param.20) | copy-start | bytes 3076
  6.5 69.2 %copy-start.13 = (f32[2048]{0:T(1024)S(1)}, f32[2048]{0:T(1024)}, u32[]{:S(2)}) copy-start(f32[2048]{0:T(1024)} %param.18) | copy-start | bytes 24580
  6.5 39.6 %all-gather.24.cloned.1.call-start = ((), (), s32[]{:S(2)}) async-start(), calls=%async_computation.10 | async-start | bytes 5242880 | tf_op jit(solution)/shard_map/all_gather | solution.py:67
  7.3 68.4 %all-gather.10.cloned.1.call-start = ((), (), s32[]{:S(2)}) async-start(), calls=%async_computation.2 | async-start | bytes 1310720 | tf_op jit(solution)/shard_map/all_gather | solution.py:71
  9.1 95.6 %all-gather.14.cloned.1.call-start = ((), (), s32[]{:S(2)}) async-start(), calls=%async_computation.4 | async-start | bytes 1310720 | tf_op jit(solution)/shard_map/all_gather | solution.py:90
  11.1 126.6 %all-gather.12.cloned.1.call-start = ((), (), s32[]{:S(2)}) async-start(), calls=%async_computation.3 | async-start | bytes 2621440 | tf_op jit(solution)/shard_map/all_gather | solution.py:89
  80.1 3.3 copy-start.12
  83.4 27.1 %copy-start.10 = (f32[1,512]{1,0:T(1,128)S(1)}, f32[1,512]{1,0:T(1,128)}, u32[]{:S(2)}) copy-start(f32[1,512]{1,0:T(1,128)} %param.24) | copy-start | bytes 6148
  106.9 28.0 %all-to-all-start = ((bf16[256,4,512]{2,0,1:T(8,128)(2,1)}), bf16[256,4,512]{2,0,1:T(8,128)(2,1)S(1)}, u32[]{:S(2)}, u32[]{:S(2)}) async-start(bf16[256,4,512]{2,0,1:T(8,128)(2,1)} %copy.23), calls=%async_computation | async-start | bytes 2097152 | tf_op jit(solution)/shard_map/all_to_all | solution.py:91
  110.5 65.3 %all-gather.16.cloned.1.call-start = ((), (), s32[]{:S(2)}) async-start(), calls=%async_computation.5 | async-start | bytes 5242880 | tf_op jit(solution)/shard_map/all_gather | solution.py:102
  137.6 3.7 copy-start.3
  140.6 2.1 copy-start.4
  142.7 141.2 %all-gather.18.cloned.1.call-start = ((), (), s32[]{:S(2)}) async-start(), calls=%async_computation.6 | async-start | bytes 7208960 | tf_op jit(solution)/shard_map/all_gather | solution.py:107
  144.0 3.5 copy-start.5
  144.1 4.8 copy-start.8
  144.1 4.9 copy-start.9
  144.1 4.9 copy-start.11
  144.1 17.0 %copy-start.6 = (f32[3,1408]{1,0:T(4,128)S(1)}, f32[3,1408]{1,0:T(4,128)}, u32[]{:S(2)}) copy-start(f32[3,1408]{1,0:T(4,128)} %param.31) | copy-start | bytes 50692
  144.1 17.0 %copy-start.7 = (f32[3,1408]{1,0:T(4,128)S(1)}, f32[3,1408]{1,0:T(4,128)}, u32[]{:S(2)}) copy-start(f32[3,1408]{1,0:T(4,128)} %param.30) | copy-start | bytes 50692
  144.1 246.3 %all-gather.20.cloned.1.call-start = ((), (), s32[]{:S(2)}) async-start(), calls=%async_computation.7 | async-start | bytes 7208960 | tf_op jit(solution)/shard_map/all_gather | solution.py:108
  147.5 136.4 %copy-start.14 = (f32[2048]{0:T(1024)S(1)}, f32[2048]{0:T(1024)}, u32[]{:S(2)}) copy-start(f32[2048]{0:T(1024)} %param.25) | copy-start | bytes 24580
  147.5 349.5 %all-gather.22.cloned.1.call-start = ((), (), s32[]{:S(2)}) async-start(), calls=%async_computation.8 | async-start | bytes 7208960 | tf_op jit(solution)/shard_map/all_gather | solution.py:121
  148.8 415.6 %reduce-scatter.2.cloned.1.call-start = ((), (), s32[]{:S(2)}) async-start(), calls=%async_computation.9 | async-start | bytes 5242880 | tf_op jit(solution)/shard_map/reduce_scatter | solution.py:126
  497.0 67.4 %copy-start.2 = (bf16[1024,512]{1,0:T(8,128)(2,1)S(1)}, bf16[1024,512]{1,0:T(8,128)(2,1)}, u32[]{:S(2)}) copy-start(bf16[1024,512]{1,0:T(8,128)(2,1)} %fusion.13) | copy-start | bytes 3145732
  497.0 69.9 %copy-start.1 = (bf16[2,128,128]{2,1,0:T(8,128)(2,1)S(1)}, bf16[2,128,128]{2,1,0:T(8,128)(2,1)}, u32[]{:S(2)}) copy-start(bf16[2,128,128]{2,1,0:T(8,128)(2,1)} %param.21) | copy-start | bytes 196612
Sparse Core Ops, SparseCore 0:
  8.9 37.1 all-gather.23
  47.7 27.9 all-gather.9
  77.3 27.3 all-gather.13
  106.1 31.4 all-gather.11
  142.8 32.9 all-gather.15
  177.2 106.6 all-gather.17
  285.5 104.9 all-gather.19
  392.0 104.9 all-gather.21
  521.8 42.6 reduce-scatter.1
where the time goes:
time: 574 us; the launch traced here: 573 us
  waiting for transfers between devices  449 us (78%)
  matrix products  58.5 us (10%)
  blocking collectives  24.1 us (4%)
  other arithmetic  19.3 us (3%)
  between operations  13.5 us (2%)
    all_gather x1, waiting for transfers between devices, shards(): lax.all_gather(gate_cast, 'fs', axis=0, tiled=True)  105 us
    all_gather x1, waiting for transfers between devices, shards(): lax.all_gather(up_cast, 'fs', axis=0, tiled=True)  94.7 us
    all_gather x1, waiting for transfers between devices, shards(): lax.all_gather(down_matrix.astype(jnp.bfloat16), 'fs', axis=1, tiled=True)  94.6 us
    reduce_scatter x1, waiting for transfers between devices, shards(): lax.psum_scatter(partial_ffn.astype(jnp.bfloat16), 'tp', scatter_dimensio...  42.8 us
    all_gather x1, waiting for transfers between devices, shards(): gathered = lax.all_gather(local_rows, 'tp', axis=1, tiled=True)  34.8 us
    all_gather x1, waiting for transfers between devices, shards(): lax.all_gather(in_matrix.astype(jnp.bfloat16), 'fs', axis=0, tiled=True)  26.5 us
    dot_general x1, matrix products, shards(): jnp.dot(hidden, lax.all_gather(down_matrix.astype(jnp.bfloat16), 'fs', ax...  24.6 us
    all_gather x1, waiting for transfers between devices, shards(): lax.all_gather(out_matrix.astype(jnp.bfloat16), 'fs', axis=1, tiled=True)  20.3 us
  transfers between devices with their start and end apart: 10, of which 10 were waited for; matrix products, arithmetic and copies ran while one was open for 9% of the time, Pallas kernels for 0%

commit v1 on v0

--- a/solution.py
+++ b/solution.py
@@ -1,3 +1,4 @@
+import functools
 import jax
 import jax.numpy as jnp
 from jax import lax
@@ -6,6 +7,26 @@
 BLOCKS = 8
 eps = 1e-06
 widest_span = 16
+
+
+def shape_ports_all(a0, join_dim):
+    piece_now = list(a0.shape[1:])
+    piece_now[join_dim] *= a0.shape[0]
+    return jnp.moveaxis(a0, 0, join_dim).reshape(piece_now)
+
+
+def _assign_packet(block_here, along_axis, dim_no):
+    parts_n = lax.axis_size(along_axis)
+    parts_seen = [block_here]
+    seen = tuple(((to_i, (to_i + 1) % parts_n) for to_i in range(parts_n)))
+    while len(parts_seen) < parts_n:
+        parts_seen.append(lax.ppermute(parts_seen[-1], along_axis, seen))
+    w2 = lax.axis_index(along_axis)
+    parts_seen = jnp.stack(parts_seen, 0)[(w2 - jnp.arange(parts_n)) % parts_n]
+    return shape_ports_all(parts_seen, dim_no)
+
+
+carry_the_rounds = functools.partial(_assign_packet, along_axis="fs", dim_no=0)
 
 
 def norm_rows(tok_rows, norm_gain):
@@ -105,7 +126,7 @@
     up_cast = up_matrix.astype(jnp.bfloat16)
     gate_full, up_full = (
         lax.all_gather(gate_cast, "fs", axis=0, tiled=True),
-        lax.all_gather(up_cast, "fs", axis=0, tiled=True),
+        carry_the_rounds(up_cast),
     )
     gate_total = jnp.dot(normed_ffn, gate_full, preferred_element_type=jnp.float32)
     up_total = jnp.dot(normed_ffn, up_full, preferred_element_type=jnp.float32)

time: 574 us -> 524 us (0.913)
  waiting for transfers between devices: 449 us -> 302 us
  blocking collectives: 24.1 us -> 86.9 us
  starting transfers between devices: 3.85 us -> 27.7 us
  local copies, waits for them, and re-layouts: 4.94 us -> 11.6 us
  other arithmetic: 19.3 us -> 25.3 us
    all_gather x1, waiting for transfers between devices: 105 us -> 0.02 us  [shards(): lax.all_gather(gate_cast, 'fs', axis=0, tiled=True)]
    ppermute x0 -> x3, waiting for transfers between devices: none -> 97.1 us  [_assign_packet(): parts_seen.append(lax.ppermute(parts_seen[-1], along_axis, seen))]
    all_gather x1 -> x0, waiting for transfers between devices: 94.7 us -> none  [shards(): lax.all_gather(up_cast, 'fs', axis=0, tiled=True)]
    all_gather x1, blocking collectives: 12.1 us -> 74.9 us  [shards(): down_cols = lax.all_gather(down_scale, 'fs', axis=1, tiled=True)]
    all_gather x1, waiting for transfers between devices: 94.6 us -> 64.5 us  [shards(): lax.all_gather(down_matrix.astype(jnp.bfloat16), 'fs', axis=1, tiled=True)]
    ppermute x0 -> x3, starting transfers between devices: none -> 23.9 us  [_assign_packet(): parts_seen.append(lax.ppermute(parts_seen[-1], along_axis, seen))]
    all_gather x1, waiting for transfers between devices: 14.5 us -> 0.01 us  [shards(): gathered_ffn = lax.all_gather(residual, 'tp', axis=1, tiled=True)]
    gather x0 -> x1, local copies, waits for them, and re-layouts: none -> 6.67 us  [_assign_packet(): parts_seen = jnp.stack(parts_seen, 0)[(w2 - jnp.arange(parts_n)) % parts_n]]
  transfers between devices with their start and end apart: 10 -> 12, of which waited for: 10 -> 9; matrix products, arithmetic and copies ran while one was open for 9% -> 12% of each run, Pallas kernels for 0% -> 0%
where the time goes in v1:
time: 524 us
  waiting for transfers between devices  302 us (58%)
  blocking collectives  86.9 us (17%)
  matrix products  56.5 us (11%)
  starting transfers between devices  27.7 us (5%)
  other arithmetic  25.3 us (5%)
  between operations  13.8 us (3%)
  local copies, waits for them, and re-layouts  11.6 us (2%)
    ppermute x3, waiting for transfers between devices, _assign_packet(): parts_seen.append(lax.ppermute(parts_seen[-1], along_axis, seen))  97.1 us
    all_gather x1, blocking collectives, shards(): down_cols = lax.all_gather(down_scale, 'fs', axis=1, tiled=True)  74.9 us
    all_gather x1, waiting for transfers between devices, shards(): lax.all_gather(down_matrix.astype(jnp.bfloat16), 'fs', axis=1, tiled=True)  64.5 us
    reduce_scatter x1, waiting for transfers between devices, shards(): lax.psum_scatter(partial_ffn.astype(jnp.bfloat16), 'tp', scatter_dimensio...  42.8 us
    all_gather x1, waiting for transfers between devices, shards(): gathered = lax.all_gather(local_rows, 'tp', axis=1, tiled=True)  34.8 us
    all_gather x1, waiting for transfers between devices, shards(): lax.all_gather(in_matrix.astype(jnp.bfloat16), 'fs', axis=0, tiled=True)  26.5 us
    dot_general x1, matrix products, shards(): jnp.dot(hidden, lax.all_gather(down_matrix.astype(jnp.bfloat16), 'fs', ax...  23.9 us
    ppermute x3, starting transfers between devices, _assign_packet(): parts_seen.append(lax.ppermute(parts_seen[-1], along_axis, seen))  23.9 us
  transfers between devices with their start and end apart: 12, of which 9 were waited for; matrix products, arithmetic and copies ran while one was open for 12% of the time, Pallas kernels for 0%

profile of v1, /device:TPU:0, one launch (start us, length us, event | category | flops | bytes accessed | tf_op | source)
XLA Modules:
  0.0 523.8 jit_solution(16956328376864459134)
XLA Ops:
  6.5 0.7 all-gather.21.cloned.1.call-update
  7.3 1.8 convert_element_type.120
  9.1 0.0 all-gather.13.cloned.1.call-start
  9.2 1.9 copy.22
  11.1 0.1 bitcast_compare_fusion.14
  11.2 0.1 broadcast_bitcast_fusion
  11.3 34.8 %all-gather.21.cloned.1.call-done = bf16[1,1024,2048]{2,1,0:T(8,128)(2,1)} async-done(((bf16[1,1024,512]{2,1,0:T(8,128)(2,1)}), bf16[1,1024,2048]{2,1,0:T(8,128)(2,1)}) %all-gather.21.cloned.1.call-update) | async-done | bytes 4194320 | tf_op jit(solution)/shard_map/all_gather | solution.py:88
  46.1 3.1 fusion.3
  49.2 26.5 %all-gather.9.cloned.1.call-done = bf16[2048,256]{1,0:T(8,128)(2,1)} async-done(((bf16[512,256]{1,0:T(8,128)(2,1)}), bf16[2048,256]{1,0:T(8,128)(2,1)}) %all-gather.9.cloned.1.call-update) | async-done | bytes 1048592 | tf_op jit(solution)/shard_map/all_gather | solution.py:92
  75.7 3.8 fusion.20
  79.5 0.1 slice.109
  79.6 0.1 slice.110
  79.7 0.1 slice.111
  79.7 0.1 slice.112
  79.8 0.1 slice.113
  79.9 0.1 slice.114
  80.0 0.1 slice.115
  80.0 0.1 slice.116
  80.1 3.2 fusion.28
  83.4 0.9 fusion.26
  84.4 20.3 %all-gather.13.cloned.1.call-done = bf16[256,2048]{0,1:T(8,128)(2,1)} async-done(((bf16[256,512]{0,1:T(8,128)(2,1)}), bf16[256,2048]{0,1:T(8,128)(2,1)}) %all-gather.13.cloned.1.call-update) | async-done | bytes 1048592 | tf_op jit(solution)/shard_map/all_gather | solution.py:111
  104.7 2.3 copy.23
  106.9 3.5 all-to-all-start
  110.5 11.9 %all_gather.31 = f32[1,2048]{1,0:T(1,128)S(1)} all-gather(f32[1,512]{1,0:T(1,128)S(1)} %copy-done.11), channel_id=1, replica_groups=mesh['grp'=2,'fs'=4,'tp'=4] {'fs'}, dimensions={1}, use_global_device_ids=true | all-gather | bytes 10240 | tf_op jit(solution)/shard_map/all_gather | solution.py:107
  122.5 12.5 %all-to-all-done = bf16[256,4,512]{2,0,1:T(8,128)(2,1)S(1)} async-done(((bf16[256,4,512]{2,0,1:T(8,128)(2,1)}), bf16[256,4,512]{2,0,1:T(8,128)(2,1)S(1)}, u32[]{:S(2)}, u32[]{:S(2)}) %all-to-all-start) | async-done | bytes 1048608 | tf_op jit(solution)/shard_map/all_to_all | solution.py:112
  135.0 2.7 all-gather.11.cloned.1.call-done
  137.6 3.0 multiply_convert_fusion.1
  140.6 0.7 convert_reduce_fusion
  141.3 1.3 fusion.13
  142.7 3.1 convert_element_type.133
  146.0 1.3 convert_element_type.136
  147.2 1.4 collective-permute-start
  148.7 1.3 convert_element_type.140
  150.0 33.0 %collective-permute-done = bf16[512,1408]{1,0:T(8,128)(2,1)} collective-permute-done((bf16[512,1408]{1,0:T(8,128)(2,1)}, bf16[512,1408]{1,0:T(8,128)(2,1)}, u32[]{:S(2)}, u32[]{:S(2)}) %collective-permute-start) | collective-permute-done | bytes 1441824 | tf_op jit(solution)/shard_map/ppermute | solution.py:23
  183.1 64.1 %collective-permute-done.1 = bf16[512,1408]{1,0:T(8,128)(2,1)} collective-permute-done((bf16[512,1408]{1,0:T(8,128)(2,1)}, bf16[512,1408]{1,0:T(8,128)(2,1)}, u32[]{:S(2)}, u32[]{:S(2)}) %collective-permute-start.1) | collective-permute-done | bytes 1441824 | tf_op jit(solution)/shard_map/ppermute | solution.py:23
  247.2 22.4 %collective-permute-start.2 = (bf16[512,1408]{1,0:T(8,128)(2,1)}, bf16[512,1408]{1,0:T(8,128)(2,1)}, u32[]{:S(2)}, u32[]{:S(2)}) collective-permute-start(bf16[512,1408]{1,0:T(8,128)(2,1)} %collective-permute-done.1), channel_id=1, source_target_pairs={{0,4},{4,8},{8,12},{12,0},{1,5},{5,9},{9,13},{13,1},{2,6},{6,10},{... | collective-permute-start | bytes 4325384 | tf_op jit(solution)/shard_map/ppermute | solution.py:23
  269.7 74.9 %all_gather.35 = f32[1,2048]{1,0:T(1,128)S(1)} all-gather(f32[1,512]{1,0:T(1,128)S(1)} %copy-done.12), channel_id=1, replica_groups=mesh['grp'=2,'fs'=4,'tp'=4] {'fs'}, dimensions={1}, use_global_device_ids=true | all-gather | bytes 10240 | tf_op jit(solution)/shard_map/all_gather | solution.py:138
  344.7 0.1 slice_reduce_fusion.2
  344.8 0.1 convert_bitcast_fusion
  344.9 5.9 %pad_maximum_fusion = bf16[4,512,1408]{2,1,0:T(8,128)(2,1)} fusion(bf16[1,512,1408]{2,1,0:T(8,128)(2,1)} %bitcast.15, bf16[1,512,1408]{2,1,0:T(8,128)(2,1)} %bitcast.14, bf16[1,512,1408]{2,1,0:T(8,128)(2,1)} %bitcast.13, bf16[1,512,1408]{2,1,0:T(8,128)(2,1)S(1)} %convert_bitcast_fusion), kind=kLoop, calls=%fused_computation.14 | loop fusion | flops 8650752 | bytes 11534336 | tf_op jit(solution)/shard_map/stack | solution.py:25
  350.8 6.7 %gather_fusion = bf16[4,512,1408]{2,1,0:T(8,128)(2,1)} fusion(bf16[4,512,1408]{2,1,0:T(8,128)(2,1)} %pad_maximum_fusion, s32[1024]{0:T(1024)S(1)} %pad_clamp_fusion), kind=kCustom, calls=%fused_computation | custom fusion | bytes 11534352 | tf_op jit(solution)/shard_map/gather | solution.py:25
  357.5 3.1 fusion
  360.7 12.1 %fusion.11 = f32[1024,1408]{1,0:T(8,128)} fusion(bf16[2048,1408]{1,0:T(8,128)(2,1)} %all-gather.17.cloned.1.call-done, f32[1408]{0:T(1024)S(1)} %reduce.1, bf16[1024,2048]{1,0:T(8,128)(2,1)} %all-gather.15.cloned.1.call-done, f32[2048]{0:T(1024)S(1)} %copy-done.15, f32[1024]{0:T(1024)S(1)} %add_rsqrt_fusion), kind=kOutput, calls=%fused_computation.22 | convolution fusion | flops 5918294016 | bytes 15746560 | tf_op jit(solution)/shard_map/dot_general | solution.py:131
  372.7 10.5 %fusion.12 = f32[1024,1408]{1,0:T(8,128)} fusion(bf16[2048,1408]{1,0:T(8,128)(2,1)} %bitcast.89, f32[1408]{0:T(1024)S(1)} %reduce.5, bf16[1024,2048]{1,0:T(8,128)(2,1)S(1)} %copy-done.4, f32[2048]{0:T(1024)S(1)} %copy-done.15, f32[1024]{0:T(1024)S(1)} %add_rsqrt_fusion), kind=kOutput, calls=%fused_computation.23 | convolution fusion | flops 5918294016 | bytes 15746560 | tf_op jit(solution)/shard_map/dot_general | solution.py:132
  383.3 64.5 %all-gather.19.cloned.1.call-done = bf16[1408,2048]{1,0:T(8,128)(2,1)} async-done(((bf16[1408,512]{1,0:T(8,128)(2,1)}), bf16[1408,2048]{1,0:T(8,128)(2,1)}) %all-gather.19.cloned.1.call-update) | async-done | bytes 5767184 | tf_op jit(solution)/shard_map/all_gather | solution.py:142
  447.7 23.9 %multiply_convert_fusion = bf16[1024,2048]{1,0:T(8,128)(2,1)} fusion(bf16[1408,2048]{1,0:T(8,128)(2,1)} %all-gather.19.cloned.1.call-done, f32[2048]{0:T(1024)S(1)} %bitcast.92, f32[1022,1408]{1,0:T(8,128)} %bitcast.98, f32[1023,1408]{1,0:T(8,128)} %bitcast.99, f32[1024,1408]{1,0:T(8,128)} %fusion.12, f32[1022,1408]{1,0:T(8,128)} %bitcast.96, ...), kind=kOutput, calls=%fused_computation.11 | convolution fusion | flops 5932843008 | bytes 44572672 | tf_op jit(solution)/shard_map/dot_general | solution.py:140
  471.7 42.8 %reduce-scatter.2.cloned.1.call-done = bf16[1024,512]{1,0:T(8,128)(2,1)} async-done(((bf16[1024,2048]{1,0:T(8,128)(2,1)}), bf16[1024,512]{1,0:T(8,128)(2,1)}) %reduce-scatter.2.cloned.1.call-update) | async-done | bytes 1048592 | tf_op jit(solution)/shard_map/reduce_scatter | solution.py:147
  514.5 2.5 fusion.25
  (61 shorter events, 0.6 us)
Async XLA Ops:
  6.5 73.6 %copy-start = (bf16[2,128,128]{2,1,0:T(8,128)(2,1)S(1)}, bf16[2,128,128]{2,1,0:T(8,128)(2,1)}, u32[]{:S(2)}) copy-start(bf16[2,128,128]{2,1,0:T(8,128)(2,1)} %param.21) | copy-start | bytes 196612
  6.5 69.2 %copy-start.16 = (f32[1,256]{1,0:T(1,128)S(1)}, f32[1,256]{1,0:T(1,128)}, u32[]{:S(2)}) copy-start(f32[1,256]{1,0:T(1,128)} %param.20) | copy-start | bytes 3076
  6.5 69.2 %copy-start.14 = (f32[2048]{0:T(1024)S(1)}, f32[2048]{0:T(1024)}, u32[]{:S(2)}) copy-start(f32[2048]{0:T(1024)} %param.18) | copy-start | bytes 24580
  6.5 39.6 %all-gather.21.cloned.1.call-start = ((), (), s32[]{:S(2)}) async-start(), calls=%async_computation.9 | async-start | bytes 5242880 | tf_op jit(solution)/shard_map/all_gather | solution.py:88
  7.3 68.4 %all-gather.9.cloned.1.call-start = ((), (), s32[]{:S(2)}) async-start(), calls=%async_computation.2 | async-start | bytes 1310720 | tf_op jit(solution)/shard_map/all_gather | solution.py:92
  9.1 95.6 %all-gather.13.cloned.1.call-start = ((), (), s32[]{:S(2)}) async-start(), calls=%async_computation.4 | async-start | bytes 1310720 | tf_op jit(solution)/shard_map/all_gather | solution.py:111
  11.1 126.6 %all-gather.11.cloned.1.call-start = ((), (), s32[]{:S(2)}) async-start(), calls=%async_computation.3 | async-start | bytes 2621440 | tf_op jit(solution)/shard_map/all_gather | solution.py:110
  80.1 3.3 copy-start.13
  83.4 27.1 %copy-start.11 = (f32[1,512]{1,0:T(1,128)S(1)}, f32[1,512]{1,0:T(1,128)}, u32[]{:S(2)}) copy-start(f32[1,512]{1,0:T(1,128)} %param.24) | copy-start | bytes 6148
  106.9 28.0 %all-to-all-start = ((bf16[256,4,512]{2,0,1:T(8,128)(2,1)}), bf16[256,4,512]{2,0,1:T(8,128)(2,1)S(1)}, u32[]{:S(2)}, u32[]{:S(2)}) async-start(bf16[256,4,512]{2,0,1:T(8,128)(2,1)} %copy.23), calls=%async_computation | async-start | bytes 2097152 | tf_op jit(solution)/shard_map/all_to_all | solution.py:112
  110.5 247.1 %all-gather.15.cloned.1.call-start = ((), (), s32[]{:S(2)}) async-start(), calls=%async_computation.5 | async-start | bytes 5242880 | tf_op jit(solution)/shard_map/all_gather | solution.py:123
  137.6 3.6 copy-start.5
  141.3 4.7 copy-start.2
  142.6 218.0 %all-gather.17.cloned.1.call-start = ((), (), s32[]{:S(2)}) async-start(), calls=%async_computation.6 | async-start | bytes 7208960 | tf_op jit(solution)/shard_map/all_gather | solution.py:128
  145.8 123.8 %copy-start.9 = (f32[1,1408]{1,0:T(1,128)S(1)}, f32[1,1408]{1,0:T(1,128)}, u32[]{:S(2)}) copy-start(f32[1,1408]{1,0:T(1,128)} %param.27) | copy-start | bytes 16900
  145.8 123.8 %copy-start.10 = (f32[1,1408]{1,0:T(1,128)S(1)}, f32[1,1408]{1,0:T(1,128)}, u32[]{:S(2)}) copy-start(f32[1,1408]{1,0:T(1,128)} %param.29) | copy-start | bytes 16900
  145.8 123.8 %copy-start.12 = (f32[1,512]{1,0:T(1,128)S(1)}, f32[1,512]{1,0:T(1,128)}, u32[]{:S(2)}) copy-start(f32[1,512]{1,0:T(1,128)} %param.33) | copy-start | bytes 6148
  145.8 198.8 %copy-start.7 = (f32[3,1408]{1,0:T(4,128)S(1)}, f32[3,1408]{1,0:T(4,128)}, u32[]{:S(2)}) copy-start(f32[3,1408]{1,0:T(4,128)} %param.31) | copy-start | bytes 50692
  145.8 198.8 %copy-start.8 = (f32[3,1408]{1,0:T(4,128)S(1)}, f32[3,1408]{1,0:T(4,128)}, u32[]{:S(2)}) copy-start(f32[3,1408]{1,0:T(4,128)} %param.30) | copy-start | bytes 50692
  145.9 301.8 %all-gather.19.cloned.1.call-start = ((), (), s32[]{:S(2)}) async-start(), calls=%async_computation.7 | async-start | bytes 7208960 | tf_op jit(solution)/shard_map/all_gather | solution.py:142
  145.9 2.7 copy-start.6
  147.2 35.8 %collective-permute-start = (bf16[512,1408]{1,0:T(8,128)(2,1)}, bf16[512,1408]{1,0:T(8,128)(2,1)}, u32[]{:S(2)}, u32[]{:S(2)}) collective-permute-start(bf16[512,1408]{1,0:T(8,128)(2,1)} %convert_element_type.136), channel_id=1, source_target_pairs={{0,4},{4,8},{8,12},{12,0},{1,5},{5,9},{9,13},{13,1},{2,6},{6,10},{... | collective-permute-start | bytes 4325384 | tf_op jit(solution)/shard_map/ppermute | solution.py:23
  150.0 364.5 %reduce-scatter.2.cloned.1.call-start = ((), (), s32[]{:S(2)}) async-start(), calls=%async_computation.8 | async-start | bytes 5242880 | tf_op jit(solution)/shard_map/reduce_scatter | solution.py:147
  183.1 64.1 %collective-permute-start.1 = (bf16[512,1408]{1,0:T(8,128)(2,1)}, bf16[512,1408]{1,0:T(8,128)(2,1)}, u32[]{:S(2)}, u32[]{:S(2)}) collective-permute-start(bf16[512,1408]{1,0:T(8,128)(2,1)} %collective-permute-done), channel_id=1, source_target_pairs={{0,4},{4,8},{8,12},{12,0},{1,5},{5,9},{9,13},{13,1},{2,6},{6,10},{... | collective-permute-start | bytes 4325384 | tf_op jit(solution)/shard_map/ppermute | solution.py:23
  247.2 97.7 %collective-permute-start.2 = (bf16[512,1408]{1,0:T(8,128)(2,1)}, bf16[512,1408]{1,0:T(8,128)(2,1)}, u32[]{:S(2)}, u32[]{:S(2)}) collective-permute-start(bf16[512,1408]{1,0:T(8,128)(2,1)} %collective-permute-done.1), channel_id=1, source_target_pairs={{0,4},{4,8},{8,12},{12,0},{1,5},{5,9},{9,13},{13,1},{2,6},{6,10},{... | collective-permute-start | bytes 4325384 | tf_op jit(solution)/shard_map/ppermute | solution.py:23
  350.8 9.8 %copy-start.15 = (f32[2048]{0:T(1024)S(1)}, f32[2048]{0:T(1024)}, u32[]{:S(2)}) copy-start(f32[2048]{0:T(1024)} %param.25) | copy-start | bytes 24580
  360.7 12.1 %copy-start.4 = (bf16[1024,2048]{1,0:T(8,128)(2,1)S(1)}, bf16[1024,2048]{1,0:T(8,128)(2,1)}, u32[]{:S(2)}) copy-start(bf16[1024,2048]{1,0:T(8,128)(2,1)} %all-gather.15.cloned.1.call-done) | copy-start | bytes 12582916
  447.7 66.8 %copy-start.3 = (bf16[1024,512]{1,0:T(8,128)(2,1)S(1)}, bf16[1024,512]{1,0:T(8,128)(2,1)}, u32[]{:S(2)}) copy-start(bf16[1024,512]{1,0:T(8,128)(2,1)} %fusion.13) | copy-start | bytes 3145732
  447.7 69.2 %copy-start.1 = (bf16[2,128,128]{2,1,0:T(8,128)(2,1)S(1)}, bf16[2,128,128]{2,1,0:T(8,128)(2,1)}, u32[]{:S(2)}) copy-start(bf16[2,128,128]{2,1,0:T(8,128)(2,1)} %param.21) | copy-start | bytes 196612
Sparse Core Ops, SparseCore 0:
  8.9 37.1 all-gather.20
  47.7 27.9 all-gather.8
  77.3 27.3 all-gather.12
  106.1 31.4 all-gather.10
  142.8 32.9 all-gather.14
  177.1 164.9 all-gather.16
  343.7 103.9 all-gather.18
  471.8 42.6 reduce-scatter.1
